TPU v7x, 32 devices: a whole 2x2x4 slice. The times are simulated.
32 devices in a mesh: sp: 8 (over z, y), tp: 4 (over x, core).
Axes of the slice: x: 2, y: 2, z: 4, core: 2. Of those that a mesh axis runs over, the one named last changes fastest.
Arguments:
- tokens: bfloat16 [4096, 2048], P(('sp', 'tp')), may hold values from -6 to 6
- queries: bfloat16 [4096, 1024], P('sp', 'tp'), may hold values from -160 to 160
- keys: bfloat16 [4096, 1024], P('sp', 'tp'), may hold values from -8 to 8
- values: bfloat16 [4096, 1024], P('sp', 'tp'), may hold values from -6 to 6
- lambdas: float32 [8], P('tp'), may hold values from 0.3 to 0.8
- head_gain: float32 [128], replicated, may hold values from 0.1 to 1.9
- out_weight: bfloat16 [1024, 2048], replicated, may hold values from -0.1875 to 0.1875
- mixer_gain: float32 [2048], replicated, may hold values from 0.1 to 1.9
- up_weight: bfloat16 [2048, 4096], P('sp', 'tp'), may hold values from -0.125 to 0.125
- down_weight: bfloat16 [4096, 2048], P('tp', 'sp'), may hold values from -0.09375 to 0.09375
Outputs:
- result: bfloat16 [4096, 2048], P(('sp', 'tp'))
All inputs are finite; a program needn't handle non-finite values.
Results may differ from a plain program's by a relative error of at most 0.02.
Values may be sent and summed in bfloat16 or wider, within the bound.
A program may use at most 128 MiB of HBM per device.

v0:
```python
import math
import jax
import jax.numpy as jnp
from jax import lax
from jax.sharding import PartitionSpec as P

DQK = 64
DV = 128


def per_device(
    tokens,
    queries,
    keys,
    values,
    lambdas,
    head_gain,
    out_weight,
    mixer_gain,
    up_weight,
    down_weight,
):
    tok_rows = queries.shape[0]
    head_count = lambdas.shape[0]
    scaling = DQK ** (-0.5)
    sp_index = lax.axis_index("sp")
    first_row = sp_index * tok_rows
    last_row = first_row + tok_rows - 1
    query_split = queries.reshape(tok_rows, head_count, 2, DQK)
    query_pos = first_row + lax.broadcasted_iota(jnp.int32, (tok_rows, 1), 0)
    floor_max = jnp.full((head_count, tok_rows), -1e30, jnp.float32)
    zero_total = jnp.zeros((head_count, tok_rows), jnp.float32)
    zero_acc = jnp.zeros((head_count, tok_rows, DV), jnp.float32)
    start_state = (floor_max, zero_total, zero_acc, floor_max, zero_total, zero_acc)
    key_piece = lax.all_gather(keys, "sp", axis=0, tiled=True)
    value_piece = lax.all_gather(values, "sp", axis=0, tiled=True)
    piece_rows = key_piece.shape[0]
    block_width = math.gcd(piece_rows, 512)

    def one_block(block_index, running):
        offset = block_index * block_width

        def update(inner):
            key_block = lax.dynamic_slice_in_dim(key_piece, offset, block_width, 0).reshape(
                block_width, head_count, 2, DQK
            )
            value_block = lax.dynamic_slice_in_dim(value_piece, offset, block_width, 0).reshape(
                block_width, head_count, DV
            )
            key_pos = offset + lax.broadcasted_iota(jnp.int32, (1, block_width), 1)
            allowed = key_pos <= query_pos
            updated = []
            for map_index in range(2):
                run_max = inner[3 * map_index]
                run_total = inner[3 * map_index + 1]
                run_acc = inner[3 * map_index + 2]
                scores = (
                    jnp.einsum(
                        "qhd,khd->hqk",
                        query_split[:, :, map_index],
                        key_block[:, :, map_index],
                        preferred_element_type=jnp.float32,
                    )
                    * scaling
                )
                scores = jnp.where(allowed[None], scores, -jnp.inf)
                new_max = jnp.maximum(run_max, jnp.max(scores, axis=2))
                shrink = jnp.exp(run_max - new_max)
                exponent = jnp.exp(scores - new_max[:, :, None])
                new_total = run_total * shrink + jnp.sum(exponent, axis=2)
                new_acc = run_acc * shrink[:, :, None] + jnp.einsum(
                    "hqk,khd->hqd",
                    exponent.astype(jnp.bfloat16),
                    value_block,
                    preferred_element_type=jnp.float32,
                )
                updated += [new_max, new_total, new_acc]
            return tuple(updated)

        return lax.cond(offset <= last_row, update, lambda inner: inner, running)

    final = lax.fori_loop(0, piece_rows // block_width, one_block, start_state)
    first_map = final[2] / final[1][:, :, None]
    second_map = final[5] / final[4][:, :, None]
    differ = first_map - lambdas[:, None, None] * second_map
    spread = lax.rsqrt(jnp.mean(differ * differ, axis=2, keepdims=True) + 1e-06)
    attended = (differ * spread * head_gain).astype(jnp.bfloat16)
    attended = jnp.transpose(attended, (1, 0, 2)).reshape(tok_rows, head_count * DV)
    all_heads = lax.all_to_all(attended, "tp", split_axis=0, concat_axis=1, tiled=True)
    projected = jnp.dot(all_heads, out_weight, preferred_element_type=jnp.float32).astype(
        jnp.bfloat16
    )
    resid = (tokens.astype(jnp.float32) + projected.astype(jnp.float32)).astype(jnp.bfloat16)
    resid_full = resid.astype(jnp.float32)
    normed = (
        resid_full
        * lax.rsqrt(jnp.mean(resid_full * resid_full, axis=1, keepdims=True) + 1e-06)
        * mixer_gain
    ).astype(jnp.bfloat16)
    up_full, down_full = (
        lax.all_gather(up_weight, "sp", axis=0, tiled=True),
        lax.all_gather(down_weight, "sp", axis=1, tiled=True),
    )
    hidden = jnp.square(
        jax.nn.relu(
            jnp.dot(
                lax.all_gather(normed, "tp", axis=0, tiled=True),
                up_full,
                preferred_element_type=jnp.float32,
            )
        )
    ).astype(jnp.bfloat16)
    mixed = lax.psum_scatter(
        jnp.dot(hidden, down_full, preferred_element_type=jnp.float32).astype(jnp.bfloat16),
        "tp",
        scatter_dimension=0,
        tiled=True,
    ).astype(jnp.float32)
    return (resid_full + mixed).astype(jnp.bfloat16)


def solution(mesh):
    placed = (
        P(("sp", "tp"), None),
        P("sp", "tp"),
        P("sp", "tp"),
        P("sp", "tp"),
        P("tp"),
        P(),
        P(),
        P(),
        P("sp", "tp"),
        P("tp", "sp"),
    )
    return jax.shard_map(
        per_device, mesh=mesh, in_specs=placed, out_specs=P(("sp", "tp"), None), check_vma=False
    )
```

profile of v0, /device:TPU:0, one launch (start us, length us, event | category | flops | bytes accessed | tf_op | source)
XLA Modules:
  0.0 390.4 jit_solution(7003081648482967234)
XLA Ops:
  6.5 1.8 copy.19
  8.4 1.8 copy.21
  10.3 1.1 copy.20
  11.4 51.1 %all-gather.6.cloned.1.call-done = bf16[4096,256]{0,1:T(8,128)(2,1)} async-done(((bf16[512,256]{0,1:T(8,128)(2,1)}), bf16[4096,256]{0,1:T(8,128)(2,1)}) %all-gather.6.cloned.1.call-update) | async-done | bytes 2097168 | tf_op jit(solution)/shard_map/all_gather | solution.py:35
  62.5 50.6 %all-gather.8.cloned.1.call-done = bf16[4096,256]{0,1:T(8,128)(2,1)} async-done(((bf16[512,256]{0,1:T(8,128)(2,1)}), bf16[4096,256]{0,1:T(8,128)(2,1)}) %all-gather.8.cloned.1.call-update) | async-done | bytes 2097168 | tf_op jit(solution)/shard_map/all_gather | solution.py:36
  113.2 6.1 %while.24 = (s32[]{:T(128)}, f32[2,512]{1,0:T(2,128)S(1)}, f32[2,512]{1,0:T(2,128)S(1)}, f32[2,512,128]{2,1,0:T(8,128)S(1)}, f32[2,512]{1,0:T(2,128)S(1)}, /*ind...) while((s32[]{:T(128)}, f32[2,512]{1,0:T(2,128)S(1)}, ...), condition=%wide.region_7.8_spmd.clone, body=%wide.region_0.7_spmd.clone.sunk | while | flops 410784768 | bytes 17707416 | solution.py:82
  113.3 5.6 %conditional.3 = ((f32[2,512]{1,0:T(2,128)S(1)}, f32[2,512]{1,0:T(2,128)S(1)}, f32[2,512,128]{2,1,0:T(8,128)S(1)}, f32[2,512]{1,0:T(2,128)S(1)}, f32[2,512]{1,0:T(2,128)S(1)}, /*index=5*/f32[2,512,128]{2,1,0:T(8,128)S(1)})) conditional(s32[]{:T(128)} %convert_element_type.94, (f32[2,512]{1,0:T(2,128)S(1)}, f32[2,512]{1,0:T(2,128)S(1)}, ...), branch_computations={%region_1.0_spmd, %region_2.6_spmd} | conditional | flops 410784768 | bytes 17705066 | solution.py:80
  113.3 1.0 constant_dynamic-slice_fusion.1
  114.5 0.6 fusion.20
  115.5 0.6 fusion.21
  116.4 1.0 constant_dynamic-slice_fusion
  117.4 0.7 convolution_add_fusion
  118.1 0.7 convolution_add_fusion.1
  120.5 8.5 %all_to_all.19 = bf16[4,128,256]{2,1,0:T(8,128)(2,1)S(1)} all-to-all(bf16[4,128,256]{2,1,0:T(8,128)(2,1)S(1)} %all_to_all.14), channel_id=1, replica_groups=mesh['sp'=8,'tp'=4] {'tp'}, dimensions={0} | all-to-all | bytes 524288 | tf_op jit(solution)/shard_map/all_to_all | solution.py:89
  129.3 3.0 multiply_reduce_fusion
  132.3 1.0 multiply_convert_fusion.1
  133.3 0.5 all-gather.12.cloned.1.call-update
  133.9 0.5 all-gather.14.cloned.1.call-update
  134.5 57.8 %all-gather.10.cloned.1.call-done = bf16[512,2048]{1,0:T(8,128)(2,1)} async-done(((bf16[128,2048]{1,0:T(8,128)(2,1)}), bf16[512,2048]{1,0:T(8,128)(2,1)}) %all-gather.10.cloned.1.call-update) | async-done | bytes 2097168 | tf_op jit(solution)/shard_map/all_gather | solution.py:107
  192.3 74.8 %all-gather.12.cloned.1.call-done = bf16[2048,1024]{1,0:T(8,128)(2,1)} async-done(((bf16[256,1024]{1,0:T(8,128)(2,1)}), bf16[2048,1024]{1,0:T(8,128)(2,1)}) %all-gather.12.cloned.1.call-update) | async-done | bytes 4194320 | tf_op jit(solution)/shard_map/all_gather | solution.py:101
  267.1 75.1 %all-gather.14.cloned.1.call-done = bf16[1024,2048]{1,0:T(8,128)(2,1)} async-done(((bf16[1024,256]{1,0:T(8,128)(2,1)}), bf16[1024,2048]{1,0:T(8,128)(2,1)}) %all-gather.14.cloned.1.call-update) | async-done | bytes 4194320 | tf_op jit(solution)/shard_map/all_gather | solution.py:102
  342.2 9.9 %convolution_convert_fusion = bf16[512,2048]{1,0:T(8,128)(2,1)} fusion(bf16[1024,2048]{1,0:T(8,128)(2,1)} %all-gather.14.cloned.1.call-done, bf16[512,2048]{1,0:T(8,128)(2,1)} %all-gather.10.cloned.1.call-done, bf16[2048,1024]{1,0:T(8,128)(2,1)} %all-gather.12.cloned.1.call-done), kind=kOutput, calls=%fused_computation.28 | convolution fusion | flops 4297588736 | bytes 12582912 | tf_op jit(solution)/shard_map/dot_general | solution.py:114
  352.1 29.5 %reduce-scatter.2.cloned.1.call-done = bf16[128,2048]{1,0:T(8,128)(2,1)} async-done(((bf16[512,2048]{1,0:T(8,128)(2,1)}), bf16[128,2048]{1,0:T(8,128)(2,1)}) %reduce-scatter.2.cloned.1.call-update) | async-done | bytes 524304 | tf_op jit(solution)/shard_map/reduce_scatter | solution.py:113
  381.6 1.9 add_convert_fusion
  (57 shorter events, 2.8 us)
Async XLA Ops:
  6.5 55.9 %all-gather.6.cloned.1.call-start = ((), (), s32[]{:S(2)}) async-start(), calls=%async_computation.2 | async-start | bytes 2359296 | tf_op jit(solution)/shard_map/all_gather | solution.py:35
  8.4 104.7 %all-gather.8.cloned.1.call-start = ((), (), s32[]{:S(2)}) async-start(), calls=%async_computation.3 | async-start | bytes 2359296 | tf_op jit(solution)/shard_map/all_gather | solution.py:36
  10.2 182.1 %all-gather.10.cloned.1.call-start = ((), (), s32[]{:S(2)}) async-start(), calls=%async_computation.4 | async-start | bytes 2621440 | tf_op jit(solution)/shard_map/all_gather | solution.py:107
  113.2 6.1 %copy-start.2 = (f32[2]{0:T(128)S(1)}, f32[2]{0:T(128)}, u32[]{:S(2)}) copy-start(f32[2]{0:T(128)} %param.18) | copy-start | bytes 28
  113.2 6.6 %copy-start.3 = (f32[128]{0:T(128)S(1)}, f32[128]{0:T(128)}, u32[]{:S(2)}) copy-start(f32[128]{0:T(128)} %param.19) | copy-start | bytes 1540
  119.3 9.9 %copy-start = (bf16[128,2048]{1,0:T(8,128)(2,1)S(1)}, bf16[128,2048]{1,0:T(8,128)(2,1)}, u32[]{:S(2)}) copy-start(bf16[128,2048]{1,0:T(8,128)(2,1)} %param.14) | copy-start | bytes 1572868
  129.3 3.0 copy-start.1
  133.3 133.8 %all-gather.12.cloned.1.call-start = ((), (), s32[]{:S(2)}) async-start(), calls=%async_computation.5 | async-start | bytes 4718592 | tf_op jit(solution)/shard_map/all_gather | solution.py:101
  133.9 208.3 %all-gather.14.cloned.1.call-start = ((), (), s32[]{:S(2)}) async-start(), calls=%async_computation.6 | async-start | bytes 4718592 | tf_op jit(solution)/shard_map/all_gather | solution.py:102
  134.5 247.2 %reduce-scatter.2.cloned.1.call-start = ((), (), s32[]{:S(2)}) async-start(), calls=%async_computation.7 | async-start | bytes 2621440 | tf_op jit(solution)/shard_map/reduce_scatter | solution.py:113
Sparse Core Ops, SparseCore 0:
  9.4 53.0 all-gather.5
  64.5 48.5 all-gather.7
  133.4 58.8 all-gather.9
  194.3 72.7 all-gather.11
  269.0 73.1 all-gather.13
  352.3 29.3 reduce-scatter.1
where the time goes:
time: 391 us; the launch traced here: 390 us
  waiting for transfers between devices  340 us (87%)
  matrix products  15.6 us (4%)
  between operations  13.6 us (3%)
  blocking collectives  8.55 us (2%)
  local copies, waits for them, and re-layouts  7.41 us (2%)
  other arithmetic  4.49 us (1%)
    all_gather x1, waiting for transfers between devices, per_device(): lax.all_gather(down_weight, 'sp', axis=1, tiled=True)  75.1 us
    all_gather x1, waiting for transfers between devices, per_device(): lax.all_gather(up_weight, 'sp', axis=0, tiled=True)  74.8 us
    all_gather x1, waiting for transfers between devices, per_device(): lax.all_gather(normed, 'tp', axis=0, tiled=True)  57.8 us
    all_gather x1, waiting for transfers between devices, per_device(): key_piece = lax.all_gather(keys, 'sp', axis=0, tiled=True)  51.1 us
    all_gather x1, waiting for transfers between devices, per_device(): value_piece = lax.all_gather(values, 'sp', axis=0, tiled=True)  50.6 us
    reduce_scatter x1, waiting for transfers between devices, per_device(): lax.psum_scatter(jnp.dot(hidden, down_full, preferred_element_type=jnp.fl...  29.5 us
    dot_general x1, matrix products, per_device(): jnp.dot(hidden, down_full, preferred_element_type=jnp.float32)  9.93 us
    all_to_all x1, blocking collectives, per_device(): lax.all_to_all(attended, 'tp', split_axis=0, concat_axis=1, tiled=True)  8.55 us
  transfers between devices with their start and end apart: 6, of which 6 were waited for; matrix products, arithmetic and copies ran while one was open for 1% of the time, Pallas kernels for 0%

commit v1 on v0

--- a/solution.py
+++ b/solution.py
@@ -3,6 +3,7 @@
 import jax.numpy as jnp
 from jax import lax
 from jax.sharding import PartitionSpec as P
+from jax.lax import all_gather
 
 DQK = 64
 DV = 128
@@ -99,7 +100,7 @@
     ).astype(jnp.bfloat16)
     up_full, down_full = (
         lax.all_gather(up_weight, "sp", axis=0, tiled=True),
-        lax.all_gather(down_weight, "sp", axis=1, tiled=True),
+        jnp.concatenate(all_gather(down_weight, axis_name="sp"), 1),
     )
     hidden = jnp.square(
         jax.nn.relu(

time: 391 us -> 333 us (0.85)
  waiting for transfers between devices: 340 us -> 276 us
  local copies, waits for them, and re-layouts: 7.41 us -> 13 us
    all_gather x1, waiting for transfers between devices: 57.8 us -> 16.1 us  [per_device(): lax.all_gather(normed, 'tp', axis=0, tiled=True)]
    all_gather x1, waiting for transfers between devices: 75.1 us -> 52.3 us  [per_device(): all_gather(down_weight, axis_name='sp')]
    reshape x0 -> x1, local copies, waits for them, and re-layouts: none -> 6.47 us  [per_device(): jnp.concatenate(all_gather(down_weight, axis_name='sp'), 1)]
  transfers between devices with their start and end apart: 6 -> 6, of which waited for: 6 -> 6; matrix products, arithmetic and copies ran while one was open for 1% -> 6% of each run, Pallas kernels for 0% -> 0%
where the time goes in v1:
time: 333 us; the launch traced here: 332 us
  waiting for transfers between devices  276 us (83%)
  matrix products  15.6 us (5%)
  between operations  13.7 us (4%)
  local copies, waits for them, and re-layouts  13 us (4%)
  blocking collectives  8.55 us (3%)
  other arithmetic  4.49 us (1%)
    all_gather x1, waiting for transfers between devices, per_device(): lax.all_gather(up_weight, 'sp', axis=0, tiled=True)  74.8 us
    all_gather x1, waiting for transfers between devices, per_device(): all_gather(down_weight, axis_name='sp')  52.3 us
    all_gather x1, waiting for transfers between devices, per_device(): key_piece = lax.all_gather(keys, 'sp', axis=0, tiled=True)  51.2 us
    all_gather x1, waiting for transfers between devices, per_device(): value_piece = lax.all_gather(values, 'sp', axis=0, tiled=True)  50.6 us
    reduce_scatter x1, waiting for transfers between devices, per_device(): lax.psum_scatter(jnp.dot(hidden, down_full, preferred_element_type=jnp.fl...  29.8 us
    all_gather x1, waiting for transfers between devices, per_device(): lax.all_gather(normed, 'tp', axis=0, tiled=True)  16.1 us
    dot_general x1, matrix products, per_device(): jnp.dot(hidden, down_full, preferred_element_type=jnp.float32)  9.9 us
    all_to_all x1, blocking collectives, per_device(): lax.all_to_all(attended, 'tp', split_axis=0, concat_axis=1, tiled=True)  8.55 us
  transfers between devices with their start and end apart: 6, of which 6 were waited for; matrix products, arithmetic and copies ran while one was open for 6% of the time, Pallas kernels for 0%

profile of v1, /device:TPU:0, one launch (start us, length us, event | category | flops | bytes accessed | tf_op | source)
XLA Modules:
  0.0 332.2 jit_solution(3469055220679544376)
XLA Ops:
  6.5 1.8 copy.31
  8.5 1.8 copy.33
  10.3 0.7 all-gather.15.cloned.1.call-update
  11.3 51.2 %all-gather.7.cloned.1.call-done = bf16[4096,256]{0,1:T(8,128)(2,1)} async-done(((bf16[512,256]{0,1:T(8,128)(2,1)}), bf16[4096,256]{0,1:T(8,128)(2,1)}) %all-gather.7.cloned.1.call-update) | async-done | bytes 2097168 | tf_op jit(solution)/shard_map/all_gather | solution.py:36
  62.5 50.6 %all-gather.9.cloned.1.call-done = bf16[4096,256]{0,1:T(8,128)(2,1)} async-done(((bf16[512,256]{0,1:T(8,128)(2,1)}), bf16[4096,256]{0,1:T(8,128)(2,1)}) %all-gather.9.cloned.1.call-update) | async-done | bytes 2097168 | tf_op jit(solution)/shard_map/all_gather | solution.py:37
  113.2 6.1 %while.24 = (s32[]{:T(128)}, f32[2,512]{1,0:T(2,128)S(1)}, f32[2,512]{1,0:T(2,128)S(1)}, f32[2,512,128]{2,1,0:T(8,128)S(1)}, f32[2,512]{1,0:T(2,128)S(1)}, /*ind...) while((s32[]{:T(128)}, f32[2,512]{1,0:T(2,128)S(1)}, ...), condition=%wide.region_7.8_spmd.clone, body=%wide.region_0.7_spmd.clone.sunk | while | flops 410784768 | bytes 17707416 | solution.py:83
  113.3 5.6 %conditional.3 = ((f32[2,512]{1,0:T(2,128)S(1)}, f32[2,512]{1,0:T(2,128)S(1)}, f32[2,512,128]{2,1,0:T(8,128)S(1)}, f32[2,512]{1,0:T(2,128)S(1)}, f32[2,512]{1,0:T(2,128)S(1)}, /*index=5*/f32[2,512,128]{2,1,0:T(8,128)S(1)})) conditional(s32[]{:T(128)} %convert_element_type.94, (f32[2,512]{1,0:T(2,128)S(1)}, f32[2,512]{1,0:T(2,128)S(1)}, ...), branch_computations={%region_1.0_spmd, %region_2.6_spmd} | conditional | flops 410784768 | bytes 17705066 | solution.py:81
  113.3 1.0 constant_dynamic-slice_fusion.1
  114.5 0.6 fusion.20
  115.5 0.6 fusion.21
  116.4 1.0 constant_dynamic-slice_fusion
  117.4 0.7 convolution_add_fusion
  118.1 0.7 convolution_add_fusion.1
  120.5 8.5 %all_to_all.19 = bf16[4,128,256]{2,1,0:T(8,128)(2,1)S(1)} all-to-all(bf16[4,128,256]{2,1,0:T(8,128)(2,1)S(1)} %all_to_all.14), channel_id=1, replica_groups=mesh['sp'=8,'tp'=4] {'tp'}, dimensions={0} | all-to-all | bytes 524288 | tf_op jit(solution)/shard_map/all_to_all | solution.py:90
  129.3 3.0 multiply_reduce_fusion
  132.3 1.0 multiply_convert_fusion.1
  133.3 0.5 all-gather.13.cloned.1.call-update
  133.9 52.3 %all-gather.15.cloned.1.call-done = bf16[8192,256]{1,0:T(8,128)(2,1)} async-done(((bf16[1024,256]{1,0:T(8,128)(2,1)}), bf16[8192,256]{1,0:T(8,128)(2,1)}) %all-gather.15.cloned.1.call-update) | async-done | bytes 4194320 | tf_op jit(solution)/shard_map/all_gather | solution.py:103
  186.2 6.5 %copy.37 = bf16[1024,8,256]{0,2,1:T(8,128)(2,1)} copy(bf16[1024,8,256]{2,0,1:T(8,128)(2,1)} %bitcast.51) | data formatting | bytes 8388608 | tf_op jit(solution)/shard_map/reshape | solution.py:103
  192.7 16.1 %all-gather.11.cloned.1.call-done = bf16[512,2048]{1,0:T(8,128)(2,1)} async-done(((bf16[128,2048]{1,0:T(8,128)(2,1)}), bf16[512,2048]{1,0:T(8,128)(2,1)}) %all-gather.11.cloned.1.call-update) | async-done | bytes 2097168 | tf_op jit(solution)/shard_map/all_gather | solution.py:108
  208.8 74.8 %all-gather.13.cloned.1.call-done = bf16[2048,1024]{1,0:T(8,128)(2,1)} async-done(((bf16[256,1024]{1,0:T(8,128)(2,1)}), bf16[2048,1024]{1,0:T(8,128)(2,1)}) %all-gather.13.cloned.1.call-update) | async-done | bytes 4194320 | tf_op jit(solution)/shard_map/all_gather | solution.py:102
  283.6 9.9 %convolution_convert_fusion = bf16[512,2048]{1,0:T(8,128)(2,1)} fusion(bf16[1024,2048]{0,1:T(8,128)(2,1)} %bitcast.52, bf16[512,2048]{1,0:T(8,128)(2,1)} %all-gather.11.cloned.1.call-done, bf16[2048,1024]{1,0:T(8,128)(2,1)} %all-gather.13.cloned.1.call-done), kind=kOutput, calls=%fused_computation.28 | convolution fusion | flops 4297588736 | bytes 12582912 | tf_op jit(solution)/shard_map/dot_general | solution.py:115
  293.5 29.8 %reduce-scatter.2.cloned.1.call-done = bf16[128,2048]{1,0:T(8,128)(2,1)} async-done(((bf16[512,2048]{1,0:T(8,128)(2,1)}), bf16[128,2048]{1,0:T(8,128)(2,1)}) %reduce-scatter.2.cloned.1.call-update) | async-done | bytes 524304 | tf_op jit(solution)/shard_map/reduce_scatter | solution.py:114
  323.4 1.9 add_convert_fusion
  (60 shorter events, 2.9 us)
Async XLA Ops:
  6.5 4.6 %copy-start.1 = (bf16[512,256]{1,0:T(8,128)(2,1)S(1)}, bf16[512,256]{1,0:T(8,128)(2,1)}, u32[]{:S(2)}) copy-start(bf16[512,256]{1,0:T(8,128)(2,1)} %param.15) | copy-start | bytes 786436
  6.5 55.9 %all-gather.7.cloned.1.call-start = ((), (), s32[]{:S(2)}) async-start(), calls=%async_computation.2 | async-start | bytes 2359296 | tf_op jit(solution)/shard_map/all_gather | solution.py:36
  8.4 104.7 %all-gather.9.cloned.1.call-start = ((), (), s32[]{:S(2)}) async-start(), calls=%async_computation.3 | async-start | bytes 2359296 | tf_op jit(solution)/shard_map/all_gather | solution.py:37
  10.3 175.9 %all-gather.15.cloned.1.call-start = ((), (), s32[]{:S(2)}) async-start(), calls=%async_computation.7 | async-start | bytes 4718592 | tf_op jit(solution)/shard_map/all_gather | solution.py:103
  11.0 197.8 %all-gather.11.cloned.1.call-start = ((), (), s32[]{:S(2)}) async-start(), calls=%async_computation.4 | async-start | bytes 2621440 | tf_op jit(solution)/shard_map/all_gather | solution.py:108
  113.2 6.1 %copy-start.3 = (f32[2]{0:T(128)S(1)}, f32[2]{0:T(128)}, u32[]{:S(2)}) copy-start(f32[2]{0:T(128)} %param.18) | copy-start | bytes 28
  113.2 6.6 %copy-start.4 = (f32[128]{0:T(128)S(1)}, f32[128]{0:T(128)}, u32[]{:S(2)}) copy-start(f32[128]{0:T(128)} %param.19) | copy-start | bytes 1540
  119.3 9.9 %copy-start = (bf16[128,2048]{1,0:T(8,128)(2,1)S(1)}, bf16[128,2048]{1,0:T(8,128)(2,1)}, u32[]{:S(2)}) copy-start(bf16[128,2048]{1,0:T(8,128)(2,1)} %param.14) | copy-start | bytes 1572868
  129.2 3.1 copy-start.2
  133.3 150.3 %all-gather.13.cloned.1.call-start = ((), (), s32[]{:S(2)}) async-start(), calls=%async_computation.5 | async-start | bytes 4718592 | tf_op jit(solution)/shard_map/all_gather | solution.py:102
  133.9 189.5 %reduce-scatter.2.cloned.1.call-start = ((), (), s32[]{:S(2)}) async-start(), calls=%async_computation.6 | async-start | bytes 2621440 | tf_op jit(solution)/shard_map/reduce_scatter | solution.py:114
Sparse Core Ops, SparseCore 0:
  9.4 53.0 all-gather.6
  64.5 48.5 all-gather.8
  115.2 70.9 all-gather.14
  187.6 21.1 all-gather.10
  210.8 72.7 all-gather.12
  293.7 29.6 reduce-scatter.1
